TPU v7x, 32 devices: a whole 2x2x4 slice. The times are simulated.
32 devices in a mesh: ep: 16 (over z, y, x), tp: 2 (over core).
Axes of the slice: x: 2, y: 2, z: 4, core: 2. Of those that a mesh axis runs over, the one named last changes fastest.
Arguments:
- tokens: bfloat16 [256, 2048], P('ep'), may hold values from -6 to 6
- recurrent_state: float32 [256, 4, 128, 256], P('ep', 'tp'), may hold values from -6 to 6
- query_weight: bfloat16 [2048, 512], P(None, 'tp'), may hold values from -0.125 to 0.125
- key_weight: bfloat16 [2048, 512], P(None, 'tp'), may hold values from -0.125 to 0.125
- decay_weight: bfloat16 [2048, 512], P(None, 'tp'), may hold values from -0.5 to 0.5
- value_weight: bfloat16 [2048, 1024], P(None, 'tp'), may hold values from -0.125 to 0.125
- gate_weight: bfloat16 [2048, 1024], P(None, 'tp'), may hold values from -0.125 to 0.125
- head_gain: float32 [256], replicated, may hold values from 0.1 to 1.9
- output_weight: bfloat16 [1024, 2048], P('tp'), may hold values from -0.375 to 0.375
- norm_gain: float32 [2, 2048], replicated, may hold values from 0.1 to 1.9
- norm_bias: float32 [2, 2048], replicated, may hold values from -1.8 to 1.8
- group_router: bfloat16 [2048, 4], replicated, may hold values from -0.125 to 0.125
- router_weight: bfloat16 [2048, 32], replicated, may hold values from -0.125 to 0.125
- routes: int32 [256, 2], P('ep'), may hold values from 0 to 31, as said below
- expert_gate: bfloat16 [32, 2048, 256], P(('ep', 'tp')), may hold values from -0.125 to 0.125
- expert_up: bfloat16 [32, 2048, 256], P(('ep', 'tp')), may hold values from -0.125 to 0.125
- expert_down: bfloat16 [32, 256, 2048], P(('ep', 'tp')), may hold values from -1.5 to 1.5
Outputs:
- new_tokens: bfloat16 [256, 2048], P('ep', 'tp')
- new_state: float32 [256, 4, 128, 256], P('ep', 'tp')
Inputs may be any that keep to these rules, and one draw needn't show every extreme that they name: `routes`: each row names two different experts of one group (group g holds the experts g * 8 to g * 8 + 7). In the rows of one device each group is named by the same number of rows and no expert by more than 2 rows; some expert is named by exactly 2 rows of every device.
All inputs are finite; a program needn't handle non-finite values.
Results may differ from a plain program's by a relative error of at most 0.01.
Values may be sent and summed in bfloat16 or wider, within the bound.
No kernel may reach another device: no remote copies, remote signals or barrier semaphores. Data moves between devices by JAX's collectives and lax.ppermute only.
A program may use at most 128 MiB of HBM per device.

v0:
```python
import jax
import jax.numpy as jnp
from jax import lax
from jax.sharding import PartitionSpec as P

alpha_res = 2.0**0.5
eps_norm = 1e-05


def layer_normed(inputs, gain_row, bias_row):
    centered = inputs - jnp.mean(inputs, axis=-1, keepdims=True)
    spread = jnp.mean(centered * centered, axis=-1, keepdims=True)
    return centered * lax.rsqrt(spread + eps_norm) * gain_row + bias_row


def on_device(
    tokens,
    recurrent_state,
    query_weight,
    key_weight,
    decay_weight,
    value_weight,
    gate_weight,
    head_gain,
    output_weight,
    norm_gain,
    norm_bias,
    group_router,
    router_weight,
    routes,
    expert_gate,
    expert_up,
    expert_down,
):
    row_count, model_width = tokens.shape
    heads_here = recurrent_state.shape[1]
    key_dim = recurrent_state.shape[2]
    value_dim = recurrent_state.shape[3]

    def project(weight):
        return jnp.dot(tokens, weight, preferred_element_type=jnp.float32)

    queries = project(query_weight).reshape(row_count, heads_here, key_dim) * key_dim ** (-0.5)
    key_rows = project(key_weight).reshape(row_count, heads_here, key_dim)
    value_rows = project(value_weight).reshape(row_count, heads_here, value_dim)
    gate_rows = project(gate_weight)
    decay_rate = jnp.exp(jax.nn.log_sigmoid(project(decay_weight)) / 16.0).reshape(
        row_count, heads_here, key_dim
    )
    new_state = (
        decay_rate[..., None] * recurrent_state + key_rows[..., None] * value_rows[:, :, None, :]
    )
    readout = jnp.sum(queries[..., None] * new_state, axis=2)
    norm_scale = lax.rsqrt(jnp.mean(readout * readout, axis=-1, keepdims=True) + eps_norm)
    gated_rows = (
        (readout * norm_scale * head_gain).reshape(row_count, heads_here * value_dim)
        * jax.nn.silu(gate_rows)
    ).astype(jnp.bfloat16)
    partial_value = jnp.dot(gated_rows, output_weight, preferred_element_type=jnp.float32)
    mixed_sum = lax.psum(partial_value.astype(jnp.bfloat16), "tp").astype(jnp.float32)
    hidden = layer_normed(
        alpha_res * tokens.astype(jnp.float32) + mixed_sum, norm_gain[0], norm_bias[0]
    ).astype(jnp.bfloat16)
    group_count = group_router.shape[1]
    expert_count = router_weight.shape[1]
    per_group = expert_count // group_count
    top_count = routes.shape[1]
    group_logit = jnp.dot(hidden, group_router, preferred_element_type=jnp.float32)
    expert_logit = jnp.dot(hidden, router_weight, preferred_element_type=jnp.float32)
    chosen_group = routes[:, 0] // per_group
    group_hit = chosen_group[:, None] == jnp.arange(group_count, dtype=jnp.int32)[None, :]
    own_logit = jnp.sum(jnp.where(group_hit, group_logit, 0.0), axis=1, keepdims=True)
    group_share = 1.0 / jnp.sum(jnp.exp(group_logit - own_logit), axis=1)
    expert_hit = routes[:, :, None] == jnp.arange(expert_count, dtype=jnp.int32)[None, None, :]
    picked = jnp.sum(jnp.where(expert_hit, expert_logit[:, None, :], 0.0), axis=2)
    route_weight = group_share[:, None] * jax.nn.sigmoid(picked - picked[:, ::-1])
    ep_count = lax.axis_size("ep")
    tp_count = lax.axis_size("tp")
    pair_index = lax.axis_index("tp")
    local_experts = expert_gate.shape[0]
    capacity = 2 * max(1, row_count // expert_count)
    total_slots = expert_count * capacity
    own_slots = total_slots // tp_count
    flat_routes = routes.reshape(row_count * top_count)
    onehot = (flat_routes[:, None] == jnp.arange(expert_count, dtype=jnp.int32)[None, :]).astype(
        jnp.int32
    )
    earlier_count = jnp.sum((jnp.cumsum(onehot, axis=0) - onehot) * onehot, axis=1)
    slot_index = flat_routes * capacity + earlier_count
    pick_all = (slot_index[:, None] == jnp.arange(total_slots, dtype=jnp.int32)[None, :]).astype(
        jnp.bfloat16
    )
    pick_mine = lax.dynamic_slice_in_dim(
        pick_all.reshape(row_count * top_count, ep_count, tp_count, local_experts * capacity),
        pair_index,
        1,
        2,
    ).reshape(row_count * top_count, own_slots)
    outgoing = jnp.einsum(
        "rks,rd->sd",
        pick_mine.reshape(row_count, top_count, own_slots),
        hidden,
        preferred_element_type=jnp.float32,
    ).astype(jnp.bfloat16)
    outgoing = outgoing.reshape(ep_count, local_experts, capacity, model_width)
    col_width = model_width // tp_count
    col_start = pair_index * col_width
    arrived = lax.all_to_all(outgoing, "ep", split_axis=0, concat_axis=0, tiled=True)
    gate_part = jnp.einsum(
        "secd,edf->secf", arrived, expert_gate, preferred_element_type=jnp.float32
    )
    up_part = jnp.einsum("secd,edf->secf", arrived, expert_up, preferred_element_type=jnp.float32)
    activation = (jax.nn.silu(gate_part) * up_part).astype(jnp.bfloat16)
    results = jnp.einsum(
        "secf,efd->secd", activation, expert_down, preferred_element_type=jnp.float32
    ).astype(jnp.bfloat16)
    returned = lax.all_to_all(
        lax.all_to_all(results, "ep", split_axis=0, concat_axis=0, tiled=True),
        "tp",
        split_axis=3,
        concat_axis=1,
        tiled=True,
    )
    fetched = jnp.dot(
        pick_all, returned.reshape(total_slots, col_width), preferred_element_type=jnp.float32
    ).reshape(row_count, top_count, col_width)
    routed_sum = jnp.sum(route_weight[..., None] * fetched, axis=1)
    blended = (
        alpha_res * lax.dynamic_slice_in_dim(hidden, col_start, col_width, 1).astype(jnp.float32)
        + routed_sum
    )
    row_total, row_squares = lax.psum(
        (jnp.sum(blended, axis=1), jnp.sum(blended * blended, axis=1)), "tp"
    )
    row_mean = row_total / model_width
    spread = row_squares / model_width - row_mean * row_mean
    gain_part = lax.dynamic_slice_in_dim(norm_gain[1], col_start, col_width, 0)
    shift_part = lax.dynamic_slice_in_dim(norm_bias[1], col_start, col_width, 0)
    new_tokens = (
        (blended - row_mean[:, None]) * lax.rsqrt(spread[:, None] + eps_norm) * gain_part
        + shift_part
    ).astype(jnp.bfloat16)
    return (new_tokens, new_state)


def solution(mesh):
    in_specs = (
        P("ep", None),
        P("ep", "tp", None, None),
        P(None, "tp"),
        P(None, "tp"),
        P(None, "tp"),
        P(None, "tp"),
        P(None, "tp"),
        P(),
        P("tp", None),
        P(),
        P(),
        P(),
        P(),
        P("ep", None),
        P(("ep", "tp"), None, None),
        P(("ep", "tp"), None, None),
        P(("ep", "tp"), None, None),
    )
    out_specs = (P("ep", "tp"), P("ep", "tp", None, None))
    return jax.shard_map(
        on_device, mesh=mesh, in_specs=in_specs, out_specs=out_specs, check_vma=False
    )
```

profile of v0, /device:TPU:0, one launch (start us, length us, event | category | flops | bytes accessed | tf_op | source)
XLA Modules:
  0.0 94.1 jit_solution(932960176985230560)
XLA Ops:
  7.2 0.0 copy-start
  7.2 0.0 copy-start.1
  7.2 0.0 copy-start.3
  7.2 0.0 all-reduce.3.cloned.1.call-start
  7.2 1.7 %convolution_multiply_fusion.1 = f32[16,256]{1,0:T(8,128)S(1)} fusion(bf16[16,2048]{1,0:T(8,128)(2,1)} %param.17, bf16[2048,256]{1,0:T(8,128)(2,1)} %param.19), kind=kOutput, calls=%fused_computation.14 | convolution fusion | flops 16781312 | bytes 1130496 | tf_op jit(solution)/shard_map/dot_general | solution.py:41
  8.9 2.0 %fusion.42 = f32[16,512]{1,0:T(8,128)S(1)} fusion(bf16[16,2048]{1,0:T(8,128)(2,1)} %param.17, bf16[2048,512]{1,0:T(8,128)(2,1)} %param.22), kind=kOutput, calls=%fused_computation.83 | convolution fusion | flops 33554432 | bytes 2195456 | tf_op jit(solution)/shard_map/dot_general | solution.py:41
  11.0 0.0 copy-done.1
  11.0 0.0 copy-done.3
  11.0 0.2 fusion.41
  11.3 1.5 %fusion.25 = f32[16,256]{1,0:T(8,128)S(1)} fusion(bf16[16,2048]{1,0:T(8,128)(2,1)S(1)} %copy-done.1, bf16[2048,256]{1,0:T(8,128)(2,1)} %param.21), kind=kOutput, calls=%fused_computation.41 | convolution fusion | flops 16814080 | bytes 1130496 | tf_op jit(solution)/shard_map/dot_general | solution.py:41
  12.8 0.0 copy-start.9
  12.8 5.7 %multiply_reduce_fusion = (f32[16,2,256]{2,1,0:T(2,128)S(1)}, f32[16,2,128,256]{3,2,1,0:T(8,128)}) fusion(f32[16,2,128]{2,1,0:T(2,128)S(1)} %mul.188, f32[16,2,256]{2,1,0:T(2,128)S(1)} %mul.195, f32[16,2,128]{2,1,0:T(2,128)S(1)} %mul.193, f32[16,2,128,256]{3,2,1,0:T(8,128)} %param.18, f32[16,2,128]{2,1,0:T(2,128)S(1)} %mul.190), kind=kLoop, calls=%fused_computation | loop fusion | flops 5234688 | bytes 8503296 | tf_op jit(solution)/shard_map/reduce_sum | solution.py:53
  18.4 0.1 multiply_reduce_fusion.3
  18.6 0.1 broadcast_multiply_fusion
  18.7 0.0 copy-done.9
  18.7 0.0 copy-done
  18.7 0.0 copy-start.7
  18.7 0.0 copy-start.5
  18.7 0.0 copy-start.6
  18.7 3.0 %convolution_convert_fusion.2 = bf16[16,2048]{1,0:T(8,128)(2,1)} fusion(bf16[512,2048]{1,0:T(8,128)(2,1)S(1)} %copy-done, f32[16,512]{1,0:T(8,128)S(1)} %bitcast.96, f32[512]{0:T(512)S(1)} %bitcast.102, bf16[16,2048]{1,0:T(8,128)(2,1)S(1)} %copy-done.1, bf16[2048,512]{1,0:T(8,128)(2,1)} %param.23), kind=kOutput, calls=%fused_computation.5 | convolution fusion | flops 67198976 | bytes 4360192 | tf_op jit(solution)/shard_map/dot_general | solution.py:59
  21.7 0.0 all-reduce.3.cloned.1.call-update
  21.8 0.0 copy-done.7
  21.8 0.1 copy.52
  21.9 0.6 fusion.34
  22.4 0.1 eq.98
  22.5 0.1 fusion.27
  22.6 0.1 reduce_window_sum.11
  22.7 0.2 select_reduce_fusion
  22.9 0.1 reduce_sum.118
  22.9 0.0 copy-done.5
  23.0 0.0 copy-done.6
  23.0 0.8 fusion.10
  23.8 1.1 %reshape.146 = f32[16,2,32]{2,1,0:T(2,128)S(1)} reshape(f32[32,16,1,2]{3,1,0,2:T(8,128)} %fusion.10) | data formatting | bytes 8192 | tf_op jit(solution)/shard_map/rks,rd->sd/convert_element_type | solution.py:99
  24.9 0.1 copy.53
  25.0 0.6 multiply_add_fusion.3
  25.6 16.7 %all-reduce.3.cloned.1.call-done = bf16[16,2048]{1,0:T(8,128)(2,1)} async-done(((bf16[16,2048]{1,0:T(8,128)(2,1)}), bf16[16,2048]{1,0:T(8,128)(2,1)}) %all-reduce.3.cloned.1.call-update) | async-done | bytes 65552 | tf_op jit(solution)/shard_map/psum | solution.py:60
  42.4 1.0 %fusion.17 = f32[16]{0:T(128)S(1)} fusion(bf16[16,2048]{1,0:T(8,128)(2,1)} %all-reduce.3.cloned.1.call-done, bf16[16,2048]{1,0:T(8,128)(2,1)S(1)} %copy-done.1), kind=kLoop, calls=%fused_computation.27 | loop fusion | flops 163824 | bytes 131136 | tf_op jit(solution)/shard_map/reduce_sum | solution.py:11
  43.3 1.0 %multiply_reduce_fusion.1 = f32[16]{0:T(128)S(1)} fusion(bf16[16,2048]{1,0:T(8,128)(2,1)} %all-reduce.3.cloned.1.call-done, bf16[16,2048]{1,0:T(8,128)(2,1)S(1)} %copy-done.1, f32[16]{0:T(128)S(1)} %broadcast_multiply_fusion.2), kind=kLoop, calls=%fused_computation.23 | loop fusion | flops 229360 | bytes 131200 | tf_op jit(solution)/shard_map/reduce_sum | solution.py:12
  44.4 0.9 add_convert_fusion
  45.3 0.2 fusion.44
  45.5 0.7 reshape.139
  46.3 6.8 %all-to-all-start = ((bf16[16,1,2,2048]{3,2,1,0:T(2,128)(2,1)}), bf16[16,1,2,2048]{3,2,1,0:T(2,128)(2,1)S(1)}, u32[]{:S(2)}, u32[]{:S(2)}) async-start(bf16[16,1,2,2048]{3,2,1,0:T(2,128)(2,1)} %bitcast.4), calls=%async_computation | async-start | bytes 262144 | tf_op jit(solution)/shard_map/all_to_all | solution.py:108
  53.1 0.9 select_reduce_fusion.2
  54.0 0.0 copy-done.4
  54.0 0.1 fusion.43
  54.2 6.8 %all-to-all-done = bf16[16,1,2,2048]{3,2,1,0:T(2,128)(2,1)S(1)} async-done(((bf16[16,1,2,2048]{3,2,1,0:T(2,128)(2,1)}), bf16[16,1,2,2048]{3,2,1,0:T(2,128)(2,1)S(1)}, u32[]{:S(2)}, u32[]{:S(2)}) %all-to-all-start) | async-done | bytes 131104 | tf_op jit(solution)/shard_map/all_to_all | solution.py:108
  61.0 1.5 %convolution_bitcast_fusion.1 = f32[16,1,2,256]{3,0,2,1:T(8,128)S(1)} fusion(bf16[1,2048,256]{2,1,0:T(8,128)(2,1)} %param.31, bf16[16,1,2,2048]{3,2,1,0:T(2,128)(2,1)S(1)} %all-to-all-done), kind=kOutput, calls=%fused_computation.10 | convolution fusion | flops 33554432 | bytes 1212416 | tf_op jit(solution)/shard_map/secd,edf->secf/dot_general | solution.py:109
  62.5 0.0 copy-done.2
  62.5 2.0 %fusion = bf16[16,1,2,2048]{3,0,2,1:T(8,128)(2,1)S(1)} fusion(bf16[1,256,2048]{2,1,0:T(8,128)(2,1)S(1)} %copy-done.2, bf16[1,2048,256]{2,1,0:T(8,128)(2,1)} %param.32, bf16[16,1,2,2048]{3,2,1,0:T(2,128)(2,1)S(1)} %all-to-all-done, f32[16,1,2,256]{3,0,2,1:T(8,128)S(1)} %convolution_bitcast_fusion.1), kind=kOutput, calls=%fused_computation.4 | convolution fusion | flops 67223552 | bytes 2392064 | tf_op jit(solution)/shard_map/secf,efd->secd/dot_general | solution.py:114
  64.4 0.8 copy.56
  65.2 3.5 %all-to-all-start.1 = ((bf16[16,1,2,2048]{3,2,1,0:T(2,128)(2,1)}), bf16[16,1,2,2048]{3,2,1,0:T(2,128)(2,1)S(1)}, u32[]{:S(2)}, u32[]{:S(2)}) async-start(bf16[16,1,2,2048]{3,2,1,0:T(2,128)(2,1)} %copy.56), calls=%async_computation.1 | async-start | bytes 262144 | tf_op jit(solution)/shard_map/all_to_all | solution.py:118
  68.8 0.2 select_reduce_fusion.1
  69.0 7.6 %all-to-all-done.1 = bf16[16,1,2,2048]{3,2,1,0:T(2,128)(2,1)S(1)} async-done(((bf16[16,1,2,2048]{3,2,1,0:T(2,128)(2,1)}), bf16[16,1,2,2048]{3,2,1,0:T(2,128)(2,1)S(1)}, u32[]{:S(2)}, u32[]{:S(2)}) %all-to-all-start.1) | async-done | bytes 131104 | tf_op jit(solution)/shard_map/all_to_all | solution.py:118
  76.5 0.8 copy.57
  77.3 0.0 copy-start.8
  77.3 1.1 %reshape.152 = bf16[2,2,16384]{2,1,0:T(2,128)(2,1)S(1)} reshape(bf16[2048,1,2,16]{3,2,1,0:T(2,128)(2,1)S(1)} %bitcast.93) | data formatting | bytes 262144
  78.4 3.8 %all_to_all.25 = bf16[2,2,16384]{2,1,0:T(2,128)(2,1)S(1)} all-to-all(bf16[2,2,16384]{2,1,0:T(2,128)(2,1)S(1)} %reshape.152), channel_id=1, replica_groups=mesh['ep'=16,'tp'=2] {'tp'}, dimensions={0} | all-to-all | bytes 262144 | tf_op jit(solution)/shard_map/all_to_all | solution.py:117
  82.2 0.7 reshape.153
  82.9 0.8 copy.58
  83.7 0.1 reshape.150
  83.7 0.2 fusion.1
  84.0 0.1 fusion.32
  84.1 2.5 %all-reduce = (f32[16]{0:T(128)S(1)}, f32[16]{0:T(128)S(1)}) all-reduce(f32[16]{0:T(128)S(1)} %get-tuple-element.3, f32[16]{0:T(128)S(1)} %get-tuple-element.2), channel_id=1, replica_groups=mesh['ep'=16,'tp'=2] {'tp'}, use_global_device_ids=true, to_apply=%region_15.16 | all-reduce | flops 32 | bytes 256 | tf_op jit(solution)/shard_map/psum | solution.py:132
  86.6 0.7 add_convert_fusion.1
  (25 shorter events, 0.3 us)
Async XLA Ops:
  7.2 11.5 %copy-start = (bf16[512,2048]{1,0:T(8,128)(2,1)S(1)}, bf16[512,2048]{1,0:T(8,128)(2,1)}, u32[]{:S(2)}) copy-start(bf16[512,2048]{1,0:T(8,128)(2,1)} %param.25) | copy-start | bytes 6291460
  7.2 3.8 %copy-start.1 = (bf16[16,2048]{1,0:T(8,128)(2,1)S(1)}, bf16[16,2048]{1,0:T(8,128)(2,1)}, u32[]{:S(2)}) copy-start(bf16[16,2048]{1,0:T(8,128)(2,1)} %param.17) | copy-start | bytes 196612
  7.2 3.8 %copy-start.3 = (bf16[2048,256]{1,0:T(8,128)(2,1)S(1)}, bf16[2048,256]{1,0:T(8,128)(2,1)}, u32[]{:S(2)}) copy-start(bf16[2048,256]{1,0:T(8,128)(2,1)} %param.20) | copy-start | bytes 3145732
  7.2 35.2 %all-reduce.3.cloned.1.call-start = ((), (), s32[]{:S(2)}) async-start(), calls=%async_computation.3 | async-start | bytes 131072 | tf_op jit(solution)/shard_map/psum | solution.py:60
  12.8 5.9 %copy-start.9 = (f32[256]{0:T(256)S(1)}, f32[256]{0:T(256)}, u32[]{:S(2)}) copy-start(f32[256]{0:T(256)} %param.24) | copy-start | bytes 3076
  18.7 3.1 %copy-start.7 = (s32[16,2]{0,1:T(2,128)S(1)}, s32[16,2]{0,1:T(2,128)}, u32[]{:S(2)}) copy-start(s32[16,2]{0,1:T(2,128)} %param.30) | copy-start | bytes 388
  18.7 4.2 %copy-start.5 = (f32[2,2048]{1,0:T(2,128)S(1)}, f32[2,2048]{1,0:T(2,128)}, u32[]{:S(2)}) copy-start(f32[2,2048]{1,0:T(2,128)} %param.27) | copy-start | bytes 49156
  18.7 4.3 %copy-start.6 = (f32[2,2048]{1,0:T(2,128)S(1)}, f32[2,2048]{1,0:T(2,128)}, u32[]{:S(2)}) copy-start(f32[2,2048]{1,0:T(2,128)} %param.26) | copy-start | bytes 49156
  21.7 32.3 %copy-start.4 = (bf16[2048,32]{0,1:T(8,128)(2,1)S(1)}, bf16[2048,32]{0,1:T(8,128)(2,1)}, u32[]{:S(2)}) copy-start(bf16[2048,32]{0,1:T(8,128)(2,1)} %param.29) | copy-start | bytes 393220
  21.7 40.8 %copy-start.2 = (bf16[1,256,2048]{2,1,0:T(8,128)(2,1)S(1)}, bf16[1,256,2048]{2,1,0:T(8,128)(2,1)}, u32[]{:S(2)}) copy-start(bf16[1,256,2048]{2,1,0:T(8,128)(2,1)} %param.33) | copy-start | bytes 3145732
  46.3 14.7 %all-to-all-start = ((bf16[16,1,2,2048]{3,2,1,0:T(2,128)(2,1)}), bf16[16,1,2,2048]{3,2,1,0:T(2,128)(2,1)S(1)}, u32[]{:S(2)}, u32[]{:S(2)}) async-start(bf16[16,1,2,2048]{3,2,1,0:T(2,128)(2,1)} %bitcast.4), calls=%async_computation | async-start | bytes 262144 | tf_op jit(solution)/shard_map/all_to_all | solution.py:108
  65.2 11.3 %all-to-all-start.1 = ((bf16[16,1,2,2048]{3,2,1,0:T(2,128)(2,1)}), bf16[16,1,2,2048]{3,2,1,0:T(2,128)(2,1)S(1)}, u32[]{:S(2)}, u32[]{:S(2)}) async-start(bf16[16,1,2,2048]{3,2,1,0:T(2,128)(2,1)} %copy.56), calls=%async_computation.1 | async-start | bytes 262144 | tf_op jit(solution)/shard_map/all_to_all | solution.py:118
  77.3 6.5 %copy-start.8 = (s32[16,2]{0,1:T(2,128)S(1)}, s32[16,2]{0,1:T(2,128)}, u32[]{:S(2)}) copy-start(s32[16,2]{0,1:T(2,128)} %multiply_add_fusion.3) | copy-start | bytes 388
Sparse Core Ops, SparseCore 0:
  21.9 20.4 all-reduce.2
where the time goes:
time: 94.9 us; the launch traced here: 94.1 us
  waiting for transfers between devices  31.1 us (33%)
  between operations  14.4 us (15%)
  matrix products  13.3 us (14%)
  other arithmetic  12.1 us (13%)
  starting transfers between devices  10.4 us (11%)
  local copies, waits for them, and re-layouts  6.53 us (7%)
  blocking collectives  6.31 us (7%)
    psum x1, waiting for transfers between devices, on_device(): lax.psum(partial_value.astype(jnp.bfloat16), 'tp').astype(jnp.float32)  16.7 us
    all_to_all x1, waiting for transfers between devices, on_device(): lax.all_to_all(results, 'ep', split_axis=0, concat_axis=0, tiled=True)  7.57 us
    all_to_all x1, starting transfers between devices, on_device(): lax.all_to_all(outgoing, 'ep', split_axis=0, concat_axis=0, tiled=True)  6.83 us
    all_to_all x1, waiting for transfers between devices, on_device(): lax.all_to_all(outgoing, 'ep', split_axis=0, concat_axis=0, tiled=True)  6.8 us
    reduce_sum x1, other arithmetic, on_device(): readout = jnp.sum(queries[..., None] * new_state, axis=2)  5.65 us
    dot_general x4, matrix products, project(): return jnp.dot(tokens, weight, preferred_element_type=jnp.float32)  5.4 us
    all_to_all x1, blocking collectives, on_device(): lax.all_to_all(lax.all_to_all(results, 'ep', split_axis=0, concat_axis=0,...  3.84 us
    all_to_all x1, starting transfers between devices, on_device(): lax.all_to_all(results, 'ep', split_axis=0, concat_axis=0, tiled=True)  3.51 us
  transfers between devices with their start and end apart: 3, of which 3 were waited for; matrix products, arithmetic and copies ran while one was open for 5% of the time, Pallas kernels for 0%

commit v1 on v0

--- a/solution.py
+++ b/solution.py
@@ -57,7 +57,9 @@
         * jax.nn.silu(gate_rows)
     ).astype(jnp.bfloat16)
     partial_value = jnp.dot(gated_rows, output_weight, preferred_element_type=jnp.float32)
-    mixed_sum = lax.psum(partial_value.astype(jnp.bfloat16), "tp").astype(jnp.float32)
+    mixed_sum = jnp.sum(lax.all_gather(partial_value.astype(jnp.bfloat16), "tp"), axis=0).astype(
+        jnp.float32
+    )
     hidden = layer_normed(
         alpha_res * tokens.astype(jnp.float32) + mixed_sum, norm_gain[0], norm_bias[0]
     ).astype(jnp.bfloat16)

time: 94.9 us -> 66.7 us (0.70)
  waiting for transfers between devices: 31.1 us -> 10.5 us
  between operations: 14.4 us -> 0.98 us
  local copies, waits for them, and re-layouts: 6.53 us -> 10.3 us
  other arithmetic: 12.1 us -> 9.87 us
  blocking collectives: 6.31 us -> 8.47 us
  starting transfers between devices: 10.4 us -> 12.3 us
    psum x1 -> x0, waiting for transfers between devices: 16.7 us -> none  [on_device(): lax.psum(partial_value.astype(jnp.bfloat16), 'tp').astype(jnp.float32)]
    all_to_all x1, waiting for transfers between devices: 6.8 us -> 2.79 us  [on_device(): lax.all_to_all(outgoing, 'ep', split_axis=0, concat_axis=0, tiled=True)]
    all_gather x0 -> x1, blocking collectives: none -> 2.17 us  [on_device(): lax.all_gather(partial_value.astype(jnp.bfloat16), 'tp')]
    slice x1, local copies, waits for them, and re-layouts: 0.01 us -> 1.5 us  [on_device(): norm_bias[0]]
    slice x1, local copies, waits for them, and re-layouts: 0.01 us -> 1.41 us  [on_device(): norm_gain[0]]
    all_to_all x1, starting transfers between devices: 6.83 us -> 8.2 us  [on_device(): lax.all_to_all(outgoing, 'ep', split_axis=0, concat_axis=0, tiled=True)]
    unnamed x26, local copies, waits for them, and re-layouts: 1.93 us -> 3.14 us
  transfers between devices with their start and end apart: 3 -> 2, of which waited for: 3 -> 2; matrix products, arithmetic and copies ran while one was open for 5% -> 8% of each run, Pallas kernels for 0% -> 0%
where the time goes in v1:
time: 66.7 us; the launch traced here: 65.9 us
  matrix products  13.4 us (20%)
  starting transfers between devices  12.3 us (18%)
  waiting for transfers between devices  10.5 us (16%)
  local copies, waits for them, and re-layouts  10.3 us (15%)
  other arithmetic  9.87 us (15%)
  blocking collectives  8.47 us (13%)
  between operations  0.98 us (1%)
    all_to_all x1, starting transfers between devices, on_device(): lax.all_to_all(outgoing, 'ep', split_axis=0, concat_axis=0, tiled=True)  8.2 us
    all_to_all x1, waiting for transfers between devices, on_device(): lax.all_to_all(results, 'ep', split_axis=0, concat_axis=0, tiled=True)  7.72 us
    reduce_sum x1, other arithmetic, on_device(): readout = jnp.sum(queries[..., None] * new_state, axis=2)  5.65 us
    dot_general x4, matrix products, project(): return jnp.dot(tokens, weight, preferred_element_type=jnp.float32)  5.26 us
    all_to_all x1, starting transfers between devices, on_device(): lax.all_to_all(results, 'ep', split_axis=0, concat_axis=0, tiled=True)  4.12 us
    all_to_all x1, blocking collectives, on_device(): lax.all_to_all(lax.all_to_all(results, 'ep', split_axis=0, concat_axis=0,...  3.84 us
    unnamed x26, local copies, waits for them, and re-layouts  3.14 us
    all_to_all x1, waiting for transfers between devices, on_device(): lax.all_to_all(outgoing, 'ep', split_axis=0, concat_axis=0, tiled=True)  2.79 us
  transfers between devices with their start and end apart: 2, of which 2 were waited for; matrix products, arithmetic and copies ran while one was open for 8% of the time, Pallas kernels for 0%

profile of v1, /device:TPU:0, one launch (start us, length us, event | category | flops | bytes accessed | tf_op | source)
XLA Modules:
  0.0 65.9 jit_solution(9486670277604851067)
XLA Ops:
  0.6 0.0 copy-start
  0.6 0.0 copy-start.1
  0.7 0.0 copy-start.3
  0.7 1.5 %fusion.38 = (f32[1,2048]{1,0:T(1,128)}, f32[1,2048]{1,0:T(1,128)}) fusion(f32[2,2048]{1,0:T(2,128)} %param.27), kind=kLoop, calls=%fused_computation.80 | loop fusion | bytes 32768 | tf_op jit(solution)/shard_map/slice | solution.py:64
  2.2 1.4 %fusion.37 = (f32[1,2048]{1,0:T(1,128)}, f32[1,2048]{1,0:T(1,128)}) fusion(f32[2,2048]{1,0:T(2,128)} %param.26), kind=kLoop, calls=%fused_computation.79 | loop fusion | bytes 32768 | tf_op jit(solution)/shard_map/slice | solution.py:64
  3.6 0.8 %copy.52 = s32[16,2]{1,0:T(8,128)S(1)} copy(s32[16,2]{0,1:T(2,128)} %param.30) | data formatting | bytes 256 | tf_op args[13]
  4.3 0.1 eq.98
  4.4 0.1 fusion.27
  4.5 0.1 reduce_window_sum.11
  4.6 0.2 select_reduce_fusion
  4.8 0.0 copy-start.8
  4.8 0.5 copy-done.8
  5.3 0.1 fusion.10
  5.4 0.2 reshape.146
  5.6 1.5 %convolution_multiply_fusion.1 = f32[16,256]{1,0:T(8,128)S(1)} fusion(bf16[16,2048]{1,0:T(8,128)(2,1)} %param.17, bf16[2048,256]{1,0:T(8,128)(2,1)} %param.19), kind=kOutput, calls=%fused_computation.14 | convolution fusion | flops 16781312 | bytes 1130496 | tf_op jit(solution)/shard_map/dot_general | solution.py:41
  7.1 2.0 %fusion.42 = f32[16,512]{1,0:T(8,128)S(1)} fusion(bf16[16,2048]{1,0:T(8,128)(2,1)} %param.17, bf16[2048,512]{1,0:T(8,128)(2,1)} %param.22), kind=kOutput, calls=%fused_computation.83 | convolution fusion | flops 33554432 | bytes 2195456 | tf_op jit(solution)/shard_map/dot_general | solution.py:41
  9.2 0.0 copy-done.1
  9.2 0.0 copy-done.3
  9.2 0.2 fusion.41
  9.5 1.5 %fusion.25 = f32[16,256]{1,0:T(8,128)S(1)} fusion(bf16[16,2048]{1,0:T(8,128)(2,1)S(1)} %copy-done.1, bf16[2048,256]{1,0:T(8,128)(2,1)} %param.21), kind=kOutput, calls=%fused_computation.41 | convolution fusion | flops 16814080 | bytes 1130496 | tf_op jit(solution)/shard_map/dot_general | solution.py:41
  11.0 0.0 copy-start.9
  11.0 5.7 %multiply_reduce_fusion = (f32[16,2,256]{2,1,0:T(2,128)S(1)}, f32[16,2,128,256]{3,2,1,0:T(8,128)}) fusion(f32[16,2,128]{2,1,0:T(2,128)S(1)} %mul.188, f32[16,2,256]{2,1,0:T(2,128)S(1)} %mul.195, f32[16,2,128]{2,1,0:T(2,128)S(1)} %mul.193, f32[16,2,128,256]{3,2,1,0:T(8,128)} %param.18, f32[16,2,128]{2,1,0:T(2,128)S(1)} %mul.190), kind=kLoop, calls=%fused_computation | loop fusion | flops 5234688 | bytes 8503296 | tf_op jit(solution)/shard_map/reduce_sum | solution.py:53
  16.7 0.1 multiply_reduce_fusion.3
  16.8 0.1 broadcast_multiply_fusion
  16.9 0.0 copy-done.9
  16.9 0.0 copy-done
  16.9 0.0 copy-start.4
  16.9 0.0 copy-start.5
  16.9 2.4 %convolution_convert_fusion.2 = bf16[16,2048]{1,0:T(8,128)(2,1)S(1)} fusion(bf16[512,2048]{1,0:T(8,128)(2,1)S(1)} %copy-done, f32[16,512]{1,0:T(8,128)S(1)} %bitcast.98, f32[512]{0:T(512)S(1)} %bitcast.104, bf16[16,2048]{1,0:T(8,128)(2,1)S(1)} %copy-done.1, bf16[2048,512]{1,0:T(8,128)(2,1)} %param.23), kind=kOutput, calls=%fused_computation.5 | convolution fusion | flops 67198976 | bytes 4360192 | tf_op jit(solution)/shard_map/dot_general | solution.py:59
  19.3 2.2 %all-gather = bf16[32,2048]{1,0:T(8,128)(2,1)S(1)} all-gather(bf16[16,2048]{1,0:T(8,128)(2,1)S(1)} %convolution_convert_fusion.2), channel_id=2, replica_groups=mesh['ep'=16,'tp'=2] {'tp'}, dimensions={0}, use_global_device_ids=true | all-gather | bytes 196608 | tf_op jit(solution)/shard_map/all_gather | solution.py:60
  21.5 0.1 fusion.17
  21.6 0.2 multiply_reduce_fusion.1
  21.9 0.0 copy-done.4
  21.9 0.0 copy-done.5
  21.9 0.1 add_convert_fusion
  22.0 0.2 fusion.44
  22.2 0.7 %reshape.139 = bf16[16,1,2,2048]{3,2,0,1:T(2,128)(2,1)} reshape(bf16[32,2048]{1,0:T(8,128)(2,1)S(1)} %fusion.44) | data formatting | bytes 262144 | tf_op jit(solution)/shard_map/reshape | solution.py:107
  22.9 8.2 %all-to-all-start = ((bf16[16,1,2,2048]{3,2,1,0:T(2,128)(2,1)}), bf16[16,1,2,2048]{3,2,1,0:T(2,128)(2,1)S(1)}, u32[]{:S(2)}, u32[]{:S(2)}) async-start(bf16[16,1,2,2048]{3,2,1,0:T(2,128)(2,1)} %bitcast.5), calls=%async_computation | async-start | bytes 262144 | tf_op jit(solution)/shard_map/all_to_all | solution.py:110
  31.2 0.7 %fusion.34 = s32[16]{0:T(128)S(1)} fusion(s32[16,2]{0,1:T(2,128)} %param.30), kind=kLoop, calls=%fused_computation.72 | loop fusion | flops 240 | bytes 128 | tf_op jit(solution)/shard_map/eq | solution.py:73
  31.9 1.0 %fusion.43 = f32[16,32]{1,0:T(8,128)S(1)} fusion(bf16[16,2048]{1,0:T(8,128)(2,1)S(1)} %add_convert_fusion, bf16[2048,32]{0,1:T(8,128)(2,1)} %param.29), kind=kOutput, calls=%fused_computation.84 | convolution fusion | flops 2097152 | bytes 198656 | tf_op jit(solution)/shard_map/dot_general | solution.py:71
  32.9 0.9 %select_reduce_fusion.2 = (f32[16]{0:T(128)S(1)}, f32[16,4]{0,1:T(4,128)S(1)}) fusion(s32[16]{0:T(128)S(1)} %fusion.34, bf16[16,2048]{1,0:T(8,128)(2,1)S(1)} %add_convert_fusion, bf16[2048,4]{0,1:T(4,128)(2,1)} %param.28), kind=kOutput, calls=%fused_computation.58 | convolution fusion | flops 262320 | bytes 82304 | tf_op jit(solution)/shard_map/dot_general | solution.py:70
  33.8 0.0 copy-start.7
  33.8 0.8 %select_reduce_fusion.1 = f32[16,2]{0,1:T(2,128)S(1)} fusion(f32[16,32]{1,0:T(8,128)S(1)} %fusion.43, s32[16,2]{0,1:T(2,128)} %param.30), kind=kLoop, calls=%fused_computation.48 | loop fusion | flops 3040 | bytes 2304 | tf_op jit(solution)/shard_map/reduce_sum | solution.py:77
  34.7 0.7 %reduce_sum.131 = s32[16,2]{1,0:T(8,128)S(1)} reshape(s32[32]{0:T(128)} %copy-done.8) | data formatting | bytes 256 | tf_op jit(solution)/shard_map/reduce_sum | solution.py:90
  35.4 0.1 copy.53
  35.5 0.7 %multiply_add_fusion.3 = s32[16,2]{0,1:T(2,128)S(1)} fusion(s32[16,2]{0,1:T(2,128)S(1)} %copy.53, s32[16,2]{0,1:T(2,128)} %param.30), kind=kLoop, calls=%fused_computation.64 | loop fusion | flops 64 | bytes 384 | tf_op jit(solution)/shard_map/add | solution.py:91
  36.2 2.8 %all-to-all-done = bf16[16,1,2,2048]{3,2,1,0:T(2,128)(2,1)S(1)} async-done(((bf16[16,1,2,2048]{3,2,1,0:T(2,128)(2,1)}), bf16[16,1,2,2048]{3,2,1,0:T(2,128)(2,1)S(1)}, u32[]{:S(2)}, u32[]{:S(2)}) %all-to-all-start) | async-done | bytes 131104 | tf_op jit(solution)/shard_map/all_to_all | solution.py:110
  39.0 1.5 %convolution_bitcast_fusion.1 = f32[16,1,2,256]{3,0,2,1:T(8,128)S(1)} fusion(bf16[1,2048,256]{2,1,0:T(8,128)(2,1)} %param.31, bf16[16,1,2,2048]{3,2,1,0:T(2,128)(2,1)S(1)} %all-to-all-done), kind=kOutput, calls=%fused_computation.10 | convolution fusion | flops 33554432 | bytes 1212416 | tf_op jit(solution)/shard_map/secd,edf->secf/dot_general | solution.py:111
  40.5 0.0 copy-done.2
  40.5 2.0 %fusion = bf16[16,1,2,2048]{3,0,2,1:T(8,128)(2,1)S(1)} fusion(bf16[1,256,2048]{2,1,0:T(8,128)(2,1)S(1)} %copy-done.2, bf16[1,2048,256]{2,1,0:T(8,128)(2,1)} %param.32, bf16[16,1,2,2048]{3,2,1,0:T(2,128)(2,1)S(1)} %all-to-all-done, f32[16,1,2,256]{3,0,2,1:T(8,128)S(1)} %convolution_bitcast_fusion.1), kind=kOutput, calls=%fused_computation.4 | convolution fusion | flops 67223552 | bytes 2392064 | tf_op jit(solution)/shard_map/secf,efd->secd/dot_general | solution.py:116
  42.4 0.8 %copy.56 = bf16[16,1,2,2048]{3,2,1,0:T(2,128)(2,1)} copy(bf16[16,1,2,2048]{3,0,2,1:T(8,128)(2,1)S(1)} %fusion) | data formatting | bytes 262144 | tf_op jit(solution)/shard_map/convert_element_type | solution.py:118
  43.2 4.1 %all-to-all-start.1 = ((bf16[16,1,2,2048]{3,2,1,0:T(2,128)(2,1)}), bf16[16,1,2,2048]{3,2,1,0:T(2,128)(2,1)S(1)}, u32[]{:S(2)}, u32[]{:S(2)}) async-start(bf16[16,1,2,2048]{3,2,1,0:T(2,128)(2,1)} %copy.56), calls=%async_computation.1 | async-start | bytes 262144 | tf_op jit(solution)/shard_map/all_to_all | solution.py:120
  47.4 0.0 copy-done.6
  47.4 7.7 %all-to-all-done.1 = bf16[16,1,2,2048]{3,2,1,0:T(2,128)(2,1)S(1)} async-done(((bf16[16,1,2,2048]{3,2,1,0:T(2,128)(2,1)}), bf16[16,1,2,2048]{3,2,1,0:T(2,128)(2,1)S(1)}, u32[]{:S(2)}, u32[]{:S(2)}) %all-to-all-start.1) | async-done | bytes 131104 | tf_op jit(solution)/shard_map/all_to_all | solution.py:120
  55.2 0.8 %copy.57 = bf16[16,1,2,2048]{0,2,1,3:T(2,128)(2,1)S(1)} copy(bf16[16,1,2,2048]{3,2,1,0:T(2,128)(2,1)S(1)} %all-to-all-done.1) | data formatting | bytes 262144 | tf_op jit(solution)/shard_map/all_to_all | solution.py:120
  55.9 1.1 %reshape.153 = bf16[2,2,16384]{2,1,0:T(2,128)(2,1)S(1)} reshape(bf16[2048,1,2,16]{3,2,1,0:T(2,128)(2,1)S(1)} %bitcast.94) | data formatting | bytes 262144
  57.0 3.8 %all_to_all.25 = bf16[2,2,16384]{2,1,0:T(2,128)(2,1)S(1)} all-to-all(bf16[2,2,16384]{2,1,0:T(2,128)(2,1)S(1)} %reshape.153), channel_id=1, replica_groups=mesh['ep'=16,'tp'=2] {'tp'}, dimensions={0} | all-to-all | bytes 262144 | tf_op jit(solution)/shard_map/all_to_all | solution.py:119
  60.8 0.7 %reshape.154 = bf16[2048,1,2,16]{3,2,1,0:T(2,128)(2,1)S(1)} reshape(bf16[2,2,16384]{2,1,0:T(2,128)(2,1)S(1)} %all_to_all.25) | data formatting | bytes 262144
  61.5 0.8 %copy.58 = bf16[16,1,2,2,1024]{4,2,3,0,1:T(2,128)(2,1)S(1)} copy(bf16[16,1,2,2,1024]{0,2,4,3,1:T(2,128)(2,1)S(1)} %bitcast.95) | data formatting | bytes 262144 | tf_op jit(solution)/shard_map/all_to_all | solution.py:119
  62.3 0.1 reshape.151
  62.4 0.2 fusion.1
  62.6 0.1 fusion.32
  62.7 2.5 %all-reduce = (f32[16]{0:T(128)S(1)}, f32[16]{0:T(128)S(1)}) all-reduce(f32[16]{0:T(128)S(1)} %get-tuple-element.3, f32[16]{0:T(128)S(1)} %get-tuple-element.2), channel_id=1, replica_groups=mesh['ep'=16,'tp'=2] {'tp'}, use_global_device_ids=true, to_apply=%region_15.16 | all-reduce | flops 32 | bytes 256 | tf_op jit(solution)/shard_map/psum | solution.py:134
  65.2 0.7 %add_convert_fusion.1 = bf16[16,1024]{1,0:T(8,128)(2,1)} fusion(f32[1024]{0:T(1024)S(1)} %bitcast.102, f32[1024]{0:T(1024)S(1)} %bitcast.103, f32[16]{0:T(128)S(1)} %get-tuple-element.13, f32[16]{0:T(128)S(1)} %get-tuple-element.12, f32[16,1024]{1,0:T(8,128)S(1)} %fusion.1, bf16[16,2048]{1,0:T(8,128)(2,1)S(1)} %add_convert_fusion, s32[]{:T(128)S(6)} %select_n.28), kind=kLoop, calls=%fused_computation.28 | loop fusion | flops 131072 | bytes 139396 | tf_op jit(solution)/shard_map/convert_element_type | solution.py:144
  (24 shorter events, 0.3 us)
Async XLA Ops:
  0.6 16.3 %copy-start = (bf16[512,2048]{1,0:T(8,128)(2,1)S(1)}, bf16[512,2048]{1,0:T(8,128)(2,1)}, u32[]{:S(2)}) copy-start(bf16[512,2048]{1,0:T(8,128)(2,1)} %param.25) | copy-start | bytes 6291460
  0.6 8.5 %copy-start.1 = (bf16[16,2048]{1,0:T(8,128)(2,1)S(1)}, bf16[16,2048]{1,0:T(8,128)(2,1)}, u32[]{:S(2)}) copy-start(bf16[16,2048]{1,0:T(8,128)(2,1)} %param.17) | copy-start | bytes 196612
  0.7 8.5 %copy-start.3 = (bf16[2048,256]{1,0:T(8,128)(2,1)S(1)}, bf16[2048,256]{1,0:T(8,128)(2,1)}, u32[]{:S(2)}) copy-start(bf16[2048,256]{1,0:T(8,128)(2,1)} %param.20) | copy-start | bytes 3145732
  4.8 0.6 copy-start.8
  11.0 5.9 %copy-start.9 = (f32[256]{0:T(256)S(1)}, f32[256]{0:T(256)}, u32[]{:S(2)}) copy-start(f32[256]{0:T(256)} %param.24) | copy-start | bytes 3076
  16.9 5.0 %copy-start.4 = (f32[1,2048]{1,0:T(1,128)S(1)}, f32[1,2048]{1,0:T(1,128)}, u32[]{:S(2)}) copy-start(f32[1,2048]{1,0:T(1,128)} %get-tuple-element.10) | copy-start | bytes 24580
  16.9 5.0 %copy-start.5 = (f32[1,2048]{1,0:T(1,128)S(1)}, f32[1,2048]{1,0:T(1,128)}, u32[]{:S(2)}) copy-start(f32[1,2048]{1,0:T(1,128)} %get-tuple-element.8) | copy-start | bytes 24580
  19.3 21.2 %copy-start.2 = (bf16[1,256,2048]{2,1,0:T(8,128)(2,1)S(1)}, bf16[1,256,2048]{2,1,0:T(8,128)(2,1)}, u32[]{:S(2)}) copy-start(bf16[1,256,2048]{2,1,0:T(8,128)(2,1)} %param.33) | copy-start | bytes 3145732
  22.9 16.0 %all-to-all-start = ((bf16[16,1,2,2048]{3,2,1,0:T(2,128)(2,1)}), bf16[16,1,2,2048]{3,2,1,0:T(2,128)(2,1)S(1)}, u32[]{:S(2)}, u32[]{:S(2)}) async-start(bf16[16,1,2,2048]{3,2,1,0:T(2,128)(2,1)} %bitcast.5), calls=%async_computation | async-start | bytes 262144 | tf_op jit(solution)/shard_map/all_to_all | solution.py:110
  33.8 13.6 %copy-start.6 = (f32[1,2048]{1,0:T(1,128)S(1)}, f32[1,2048]{1,0:T(1,128)}, u32[]{:S(2)}) copy-start(f32[1,2048]{1,0:T(1,128)} %get-tuple-element.11) | copy-start | bytes 24580
  33.8 13.6 %copy-start.7 = (f32[1,2048]{1,0:T(1,128)S(1)}, f32[1,2048]{1,0:T(1,128)}, u32[]{:S(2)}) copy-start(f32[1,2048]{1,0:T(1,128)} %get-tuple-element.9) | copy-start | bytes 24580
  43.2 11.9 %all-to-all-start.1 = ((bf16[16,1,2,2048]{3,2,1,0:T(2,128)(2,1)}), bf16[16,1,2,2048]{3,2,1,0:T(2,128)(2,1)S(1)}, u32[]{:S(2)}, u32[]{:S(2)}) async-start(bf16[16,1,2,2048]{3,2,1,0:T(2,128)(2,1)} %copy.56), calls=%async_computation.1 | async-start | bytes 262144 | tf_op jit(solution)/shard_map/all_to_all | solution.py:120
